TPU v7x, 32 devices: a whole 2x2x4 slice. The times are simulated.
32 devices in a mesh: sp: 4 (over y, x), tp: 8 (over z, core).
Axes of the slice: x: 2, y: 2, z: 4, core: 2. Of those that a mesh axis runs over, the one named last changes fastest.
Arguments:
- saved_input: bfloat16 [1024, 2048], P('sp'), may hold values from -6 to 6
- cotangent: bfloat16 [1024, 2048], P('sp'), may hold values from -6 to 6
- expert_ids: int32 [1024, 2], P('sp'), may hold values from 0 to 3, all different within a row; in each aligned block of 256 rows (0 to 255, 256 to 511, ...) at most 256 rows name the same one
- route_weight: float32 [1024, 2], P('sp'), may hold values from 0.1 to 0.9
- w_gate: bfloat16 [4, 2048, 6144], P('sp', None, 'tp'), may hold values from -0.125 to 0.125
- w_up: bfloat16 [4, 2048, 6144], P('sp', None, 'tp'), may hold values from -0.125 to 0.125
- w_down: bfloat16 [4, 6144, 2048], P('sp', 'tp'), may hold values from -0.078125 to 0.078125
- w_out: bfloat16 [2048, 2048], P(None, 'tp'), may hold values from -0.125 to 0.125
- channel_gain: float32 [2048], P('tp'), may hold values from 0.1 to 1.9
- conv_taps: float32 [31, 2048], P(None, 'tp'), may hold values from -1 to 1
- glu_value: bfloat16 [2048, 1024], P('tp', 'sp'), may hold values from -6 to 6
- glu_gate: bfloat16 [2048, 1024], P('tp', 'sp'), may hold values from -8 to 8
- conv_out: bfloat16 [2048, 1024], P('tp', 'sp'), may hold values from -6 to 6
- norm_mean: float32 [1024], P('sp'), may hold values from -3 to 3
- norm_rstd: float32 [1024], P('sp'), may hold values from 0.5 to 2
Outputs:
- gate_grad: bfloat16 [4, 2048, 6144], P('sp', None, 'tp')
- up_grad: bfloat16 [4, 2048, 6144], P('sp', None, 'tp')
- down_grad: bfloat16 [4, 6144, 2048], P('sp', 'tp')
- proj_grad: float32 [2048, 2048], P('sp', 'tp')
- value_grad: bfloat16 [2048, 1024], P('tp', 'sp')
- gate_in_grad: bfloat16 [2048, 1024], P('tp', 'sp')
Inputs may be any that keep to these rules, and one draw needn't show every extreme that they name: `expert_ids`: the two experts of a position differ. In the positions of one block of 256, no expert is named more than 256 times, a bound that some block reaches.
All inputs are finite; a program needn't handle non-finite values.
Results may differ from a plain program's by a relative error of at most 0.018.
Values may be sent and summed in bfloat16 or wider, within the bound.
A program may use at most 128 MiB of HBM per device.

v0:
```python
import jax
import jax.numpy as jnp
from jax import lax
from jax.sharding import PartitionSpec as P

D = 2048
C = 2048


def from_behind(value, axis, by):
    devices = lax.axis_size(axis)
    pairs = [(i, i + by) for i in range(devices) if 0 <= i + by < devices]
    return lax.ppermute(value, axis, pairs)


def contract(left, right, left_dim, right_dim):
    return lax.dot_general(
        left, right, (((left_dim,), (right_dim,)), ((), ())), preferred_element_type=jnp.float32
    )


def expert_grads(rows_in, rows_cot, gate_weight, up_weight, down_weight):
    gate_pre = jnp.dot(rows_in, gate_weight, preferred_element_type=jnp.float32)
    up_pre = jnp.dot(rows_in, up_weight, preferred_element_type=jnp.float32)
    sigma = jax.nn.sigmoid(gate_pre)
    hidden = (gate_pre * sigma * up_pre).astype(jnp.bfloat16)
    hidden_cot = contract(rows_cot, down_weight, 1, 1)
    down_part = contract(hidden, rows_cot, 0, 0).astype(jnp.bfloat16)
    gate_cot = (hidden_cot * up_pre * sigma * (1.0 + gate_pre * (1.0 - sigma))).astype(jnp.bfloat16)
    up_cot = (hidden_cot * gate_pre * sigma).astype(jnp.bfloat16)
    gate_part = contract(rows_in, gate_cot, 0, 0).astype(jnp.bfloat16)
    up_part = contract(rows_in, up_cot, 0, 0).astype(jnp.bfloat16)
    input_cot = contract(gate_cot, gate_weight, 1, 1) + contract(up_cot, up_weight, 1, 1)
    return (gate_part, up_part, down_part, input_cot)


def on_device(
    saved_input,
    cotangent,
    expert_ids,
    route_weight,
    w_gate,
    w_up,
    w_down,
    w_out,
    channel_gain,
    conv_taps,
    glu_value,
    glu_gate,
    conv_out,
    norm_mean,
    norm_rstd,
):
    tokens_here = cotangent.shape[0]
    sp_count = lax.axis_size("sp")
    local_experts = w_gate.shape[0]
    expert_count = local_experts * sp_count
    capacity = 4 * tokens_here // expert_count
    pairs = expert_ids.reshape(2 * tokens_here)
    onehot = (pairs[:, None] == jnp.arange(expert_count, dtype=jnp.int32)[None, :]).astype(
        jnp.int32
    )
    before = jnp.cumsum(onehot, axis=0) - onehot
    target = pairs * capacity + jnp.sum(before * onehot, axis=1)
    owner = (
        jnp.zeros((expert_count * capacity,), jnp.int32)
        .at[target]
        .set(jnp.arange(2 * tokens_here, dtype=jnp.int32) + 1)
    )
    filled = (owner > 0)[:, None]
    pair_index = jnp.maximum(owner - 1, 0)
    scaled = (route_weight[:, :, None] * cotangent.astype(jnp.float32)[:, None, :]).astype(
        jnp.bfloat16
    )
    scaled = scaled.reshape(2 * tokens_here, D)
    send_cot = jnp.where(filled, scaled[pair_index], jnp.zeros_like(scaled[:1])).reshape(
        expert_count, capacity, D
    )
    send_in = jnp.where(filled, saved_input[pair_index // 2], jnp.zeros_like(saved_input[:1]))
    send_in = send_in.reshape(expert_count, capacity, D)
    rows_cot, rows_in = (
        lax.all_to_all(send_cot, "sp", split_axis=0, concat_axis=1, tiled=True),
        lax.all_to_all(send_in, "sp", split_axis=0, concat_axis=1, tiled=True),
    )
    results = [expert_grads(rows_in[0], rows_cot[0], w_gate[0], w_up[0], w_down[0])]
    gate_grad = jnp.stack([result[0] for result in results])
    up_grad = jnp.stack([result[1] for result in results])
    down_grad = jnp.stack([result[2] for result in results])
    input_cot = jnp.stack([result[3] for result in results])
    blocks = input_cot.reshape(local_experts, sp_count, capacity, D)
    share = lax.psum_scatter(
        blocks.astype(jnp.bfloat16), "tp", scatter_dimension=2, tiled=True
    ).astype(jnp.float32)
    returned = lax.all_to_all(
        share.astype(jnp.bfloat16), "sp", split_axis=1, concat_axis=0, tiled=True
    ).astype(share.dtype)
    whole = lax.all_gather(returned.astype(jnp.bfloat16), "tp", axis=2, tiled=True).astype(
        returned.dtype
    )
    routed = whole.reshape(expert_count * capacity, D)[target].reshape(tokens_here, 2, D)
    summed = jnp.sum(routed, axis=1)
    mixed_cot = (cotangent.astype(jnp.float32) + summed).astype(jnp.bfloat16)
    centered = (conv_out.astype(jnp.float32) - norm_mean[None, :]) * norm_rstd[None, :]
    normed = centered * channel_gain[:, None]
    sigma = jax.nn.sigmoid(normed)
    output_act = (normed * sigma).astype(jnp.bfloat16)
    proj_grad = lax.psum_scatter(
        contract(mixed_cot, output_act, 0, 1).astype(jnp.bfloat16),
        "sp",
        scatter_dimension=0,
        tiled=True,
    ).astype(jnp.float32)
    act_cot = contract(w_out, mixed_cot, 0, 1)
    norm_cot = act_cot * sigma * (1.0 + normed * (1.0 - sigma)) * channel_gain[:, None]
    first_sum, second_sum = lax.psum(
        (jnp.sum(norm_cot, axis=0), jnp.sum(norm_cot * centered, axis=0)), "tp"
    )
    conv_cot = norm_rstd[None, :] * (
        norm_cot - first_sum[None, :] / C - centered * second_sum[None, :] / C
    )
    reach = conv_taps.shape[0] - 1
    rim = from_behind(conv_cot[:, :reach], "sp", -1)
    padded = jnp.concatenate([conv_cot, rim], axis=1)
    glu_cot = conv_taps[0][:, None] * padded[:, :tokens_here]
    for lag in range(1, reach + 1):
        glu_cot = glu_cot + conv_taps[lag][:, None] * padded[:, lag : lag + tokens_here]
    gate_sigma = jax.nn.sigmoid(glu_gate.astype(jnp.float32))
    value_grad = (glu_cot * gate_sigma).astype(jnp.bfloat16)
    gate_in_grad = (
        glu_cot * glu_value.astype(jnp.float32) * gate_sigma * (1.0 - gate_sigma)
    ).astype(jnp.bfloat16)
    return (gate_grad, up_grad, down_grad, proj_grad, value_grad, gate_in_grad)


def solution(mesh):
    in_specs = (
        P("sp", None),
        P("sp", None),
        P("sp", None),
        P("sp", None),
        P("sp", None, "tp"),
        P("sp", None, "tp"),
        P("sp", "tp", None),
        P(None, "tp"),
        P("tp"),
        P(None, "tp"),
        P("tp", "sp"),
        P("tp", "sp"),
        P("tp", "sp"),
        P("sp"),
        P("sp"),
    )
    out_specs = (
        P("sp", None, "tp"),
        P("sp", None, "tp"),
        P("sp", "tp", None),
        P("sp", "tp"),
        P("tp", "sp"),
        P("tp", "sp"),
    )
    return jax.shard_map(
        on_device, mesh=mesh, in_specs=in_specs, out_specs=out_specs, check_vma=False
    )
```

profile of v0, /device:TPU:4, one launch (start us, length us, event | category | flops | bytes accessed | tf_op | source)
XLA Modules:
  0.0 370.3 jit_solution(1634541059612848329)
XLA Ops:
  9.5 1.2 reduce-window.6
  11.3 2.4 scatter_custom_fusion
  14.7 5.3 %mul.440 = f32[256,2,2048]{2,1,0:T(2,128)} broadcast(bf16[256,2048]{1,0:T(8,128)(2,1)} %param.16), dimensions={0,2} | broadcast | bytes 5242880 | tf_op jit(solution)/shard_map/mul | solution.py:72
  20.1 6.2 %mul.441 = f32[512,2048]{1,0:T(8,128)} reshape(f32[256,2,2048]{2,1,0:T(2,128)} %mul.440) | data formatting | bytes 8388608 | tf_op jit(solution)/shard_map/mul | solution.py:72
  26.2 10.2 %gather_fusion = bf16[1024,2048]{1,0:T(8,128)(2,1)} fusion(bf16[256,2048]{1,0:T(8,128)(2,1)} %param.15, s32[1024]{0:T(1024)S(1)} %get-tuple-element.64), kind=kCustom, calls=%fused_computation | custom fusion | bytes 8392704 | tf_op jit(solution)/shard_map/gather | solution.py:79
  36.4 3.8 %multiply_convert_fusion = bf16[512,2048]{1,0:T(8,128)(2,1)} fusion(f32[512,2048]{1,0:T(8,128)} %mul.441, f32[512]{0:T(512)S(1)} %mul.438), kind=kLoop, calls=%fused_computation.6 | loop fusion | flops 2097152 | bytes 6293504 | tf_op jit(solution)/shard_map/convert_element_type | solution.py:72
  40.2 10.7 %gather_fusion.1 = bf16[1024,2048]{1,0:T(8,128)(2,1)} fusion(bf16[512,2048]{1,0:T(8,128)(2,1)} %multiply_convert_fusion, s32[1024]{0:T(1024)S(1)} %get-tuple-element.63), kind=kCustom, calls=%fused_computation.1 | custom fusion | bytes 8392704 | tf_op jit(solution)/shard_map/gather | solution.py:76
  50.9 5.2 %broadcast_select_fusion = (bf16[4,256,2048]{2,1,0:T(8,128)(2,1)}, bf16[4,256,2048]{2,1,0:T(8,128)(2,1)S(1)}) fusion(bf16[4,256,2048]{2,1,0:T(8,128)(2,1)} %bitcast.104, pred[4,256]{1,0:T(4,128)(4,1)S(1)} %broadcast_in_dim.43, bf16[4,256,2048]{2,1,0:T(8,128)(2,1)} %bitcast.103), kind=kLoop, calls=%fused_computation.7 | loop fusion | flops 4194304 | bytes 16778240 | tf_op jit(solution)/shard_map/jit(_where)/select_n | solution.py:76
  56.1 50.8 %all_to_all.30 = bf16[4,256,2048]{2,1,0:T(8,128)(2,1)} all-to-all(bf16[4,256,2048]{2,1,0:T(8,128)(2,1)S(1)} %get-tuple-element.66), channel_id=1, replica_groups=mesh['sp'=4,'tp'=8] {'sp'}, dimensions={0} | all-to-all | bytes 8388608 | tf_op jit(solution)/shard_map/all_to_all | solution.py:83
  107.0 5.9 %all-to-all-start.1 = ((bf16[4,256,2048]{2,1,0:T(8,128)(2,1)}), bf16[4,256,2048]{2,1,0:T(8,128)(2,1)}, u32[]{:S(2)}, u32[]{:S(2)}) async-start(bf16[4,256,2048]{2,1,0:T(8,128)(2,1)} %get-tuple-element.65), calls=%async_computation.1 | async-start | bytes 8388608 | tf_op jit(solution)/shard_map/all_to_all | solution.py:82
  113.3 7.4 %fusion.2 = f32[1024,768]{1,0:T(8,128)} fusion(bf16[1024,2048]{1,0:T(8,128)(2,1)} %bitcast.105, bf16[1,2048,768]{2,1,0:T(8,128)(2,1)S(1)} %copy-done), kind=kOutput, calls=%fused_computation.43 | convolution fusion | flops 3221225472 | bytes 10485760 | tf_op jit(solution)/shard_map/dot_general | solution.py:23
  120.7 5.1 %fusion.5 = f32[1024,768]{1,0:T(8,128)} fusion(bf16[1024,2048]{1,0:T(8,128)(2,1)S(1)} %bitcast.108, bf16[1,2048,768]{2,1,0:T(8,128)(2,1)S(1)} %copy-done.41), kind=kOutput, calls=%fused_computation.46 | convolution fusion | flops 3221225472 | bytes 10485760 | tf_op jit(solution)/shard_map/dot_general | solution.py:24
  125.8 32.8 %all-to-all-done.1 = bf16[4,256,2048]{2,1,0:T(8,128)(2,1)} async-done(((bf16[4,256,2048]{2,1,0:T(8,128)(2,1)}), bf16[4,256,2048]{2,1,0:T(8,128)(2,1)}, u32[]{:S(2)}, u32[]{:S(2)}) %all-to-all-start.1) | async-done | bytes 4194336 | tf_op jit(solution)/shard_map/all_to_all | solution.py:82
  158.6 9.2 %multiply_convert_fusion.2 = (bf16[1024,768]{1,0:T(8,128)(2,1)S(1)}, bf16[1024,768]{1,0:T(8,128)(2,1)S(1)}) fusion(f32[1024,768]{1,0:T(8,128)} %fusion.2, f32[1024,768]{1,0:T(8,128)} %fusion.5, bf16[1024,2048]{1,0:T(8,128)(2,1)} %bitcast.6, bf16[1,768,2048]{2,1,0:T(8,128)(2,1)} %param.21), kind=kOutput, calls=%fused_computation.51 | convolution fusion | flops 3231449088 | bytes 16777216 | tf_op jit(solution)/shard_map/dot_general | solution.py:17
  167.8 3.4 fusion
  171.3 17.2 %add_convert_fusion = bf16[1024,2048]{1,0:T(8,128)(2,1)} fusion(f32[1024,2048]{1,0:T(8,128)S(1)} %fusion, bf16[1024,768]{1,0:T(8,128)(2,1)S(1)} %get-tuple-element.30, bf16[1,2048,768]{2,1,0:T(8,128)(2,1)S(1)} %copy-done.42), kind=kOutput, calls=%fused_computation.4 | convolution fusion | flops 3225419776 | bytes 17301504 | tf_op jit(solution)/shard_map/dot_general | solution.py:17
  188.5 50.3 %reduce-scatter.3.cloned.1.call-done = bf16[1,4,32,2048]{3,2,0,1:T(8,128)(2,1)} async-done(((bf16[1,4,256,2048]{3,2,0,1:T(8,128)(2,1)}), bf16[1,4,32,2048]{3,2,0,1:T(8,128)(2,1)}) %reduce-scatter.3.cloned.1.call-update) | async-done | bytes 524304 | tf_op jit(solution)/shard_map/reduce_scatter | solution.py:91
  238.8 10.8 %all_to_all.31 = bf16[1,4,32,2048]{3,2,0,1:T(8,128)(2,1)} all-to-all(bf16[1,4,32,2048]{3,2,0,1:T(8,128)(2,1)} %reduce-scatter.3.cloned.1.call-done), channel_id=1, replica_groups=mesh['sp'=4,'tp'=8] {'sp'}, dimensions={1} | all-to-all | bytes 1048576 | tf_op jit(solution)/shard_map/all_to_all | solution.py:94
  251.4 7.5 %fusion.10 = bf16[1,2048,768]{2,1,0:T(8,128)(2,1)} fusion(bf16[1024,2048]{1,0:T(8,128)(2,1)} %bitcast.106, bf16[1024,768]{1,0:T(8,128)(2,1)S(1)} %copy-done.47), kind=kOutput, calls=%fused_computation.55 | convolution fusion | flops 3222798336 | bytes 8912896 | tf_op jit(solution)/shard_map/dot_general | solution.py:17
  258.9 7.3 %fusion.11 = bf16[1,768,2048]{2,1,0:T(8,128)(2,1)} fusion(bf16[1024,2048]{1,0:T(8,128)(2,1)} %bitcast.6, f32[1024,768]{1,0:T(8,128)S(1)} %copy-done.44, f32[1024,768]{1,0:T(8,128)S(1)} %copy-done.43), kind=kOutput, calls=%fused_computation.56 | convolution fusion | flops 3227516928 | bytes 13631488 | tf_op jit(solution)/shard_map/dot_general | solution.py:17
  266.2 29.7 %all-gather.3.cloned.1.call-done = bf16[1,4,256,2048]{3,2,0,1:T(8,128)(2,1)} async-done(((bf16[1,4,32,2048]{3,2,0,1:T(8,128)(2,1)}), bf16[1,4,256,2048]{3,2,0,1:T(8,128)(2,1)}) %all-gather.3.cloned.1.call-update) | async-done | bytes 4194320 | tf_op jit(solution)/shard_map/all_gather | solution.py:97
  295.9 6.5 %bitcast_convert_fusion = f32[1024,2048]{1,0:T(8,128)} fusion(bf16[1,4,256,2048]{3,2,0,1:T(8,128)(2,1)} %all-gather.3.cloned.1.call-done), kind=kLoop, calls=%fused_computation.5 | loop fusion | flops 2097152 | bytes 12582912 | tf_op jit(solution)/shard_map/reshape | solution.py:100
  302.4 8.8 %gather_fusion.2 = f32[512,2048]{1,0:T(8,128)} fusion(f32[1024,2048]{1,0:T(8,128)} %bitcast_convert_fusion, s32[1024]{0:T(1024)S(1)} %pad_clamp_fusion), kind=kCustom, calls=%fused_computation.2 | custom fusion | bytes 8390656 | tf_op jit(solution)/shard_map/gather | solution.py:100
  311.2 5.8 %reshape.157 = f32[256,2,2048]{2,1,0:T(2,128)} reshape(f32[512,2048]{1,0:T(8,128)} %gather_fusion.2) | data formatting | bytes 8388608 | tf_op jit(solution)/shard_map/reshape | solution.py:100
  317.0 7.3 %reduce_sum.40 = f32[256,2048]{1,0:T(8,128)S(1)} reduce(f32[256,2,2048]{2,1,0:T(2,128)} %reshape.157, f32[]{:T(128)} %constant.43.clone.1), dimensions={1}, to_apply=%region_5.6 | reduce | flops 524288 | bytes 6291460 | tf_op jit(solution)/shard_map/reduce_sum | solution.py:101
  324.4 1.7 convolution_convert_fusion.3
  326.1 3.0 fusion.121
  329.1 14.7 %all-reduce = (f32[256]{0:T(256)S(1)}, f32[256]{0:T(256)S(1)}) all-reduce(f32[256]{0:T(256)} %get-tuple-element.25, f32[256]{0:T(256)} %get-tuple-element.24), channel_id=1, replica_groups=mesh['sp'=4,'tp'=8] {'tp'}, use_global_device_ids=true, to_apply=%region_10.11 | all-reduce | flops 512 | bytes 4096 | tf_op jit(solution)/shard_map/psum | solution.py:115
  345.2 3.5 collective-permute-start
  348.8 8.0 %fusion.9 = bf16[1,2048,768]{2,1,0:T(8,128)(2,1)} fusion(bf16[1024,2048]{1,0:T(8,128)(2,1)} %bitcast.107, bf16[1024,768]{1,0:T(8,128)(2,1)} %copy-done.45), kind=kOutput, calls=%fused_computation.54 | convolution fusion | flops 3222798336 | bytes 8912896 | tf_op jit(solution)/shard_map/dot_general | solution.py:17
  357.1 2.1 multiply_convert_fusion.5
  361.8 1.8 convert_element_type.95
  (134 shorter events, 9.8 us)
Async XLA Ops:
  7.2 106.1 %copy-start = (bf16[1,2048,768]{2,1,0:T(8,128)(2,1)S(1)}, bf16[1,2048,768]{2,1,0:T(8,128)(2,1)}, u32[]{:S(2)}) copy-start(bf16[1,2048,768]{2,1,0:T(8,128)(2,1)} %param.19) | copy-start | bytes 9437188
  107.0 51.6 %all-to-all-start.1 = ((bf16[4,256,2048]{2,1,0:T(8,128)(2,1)}), bf16[4,256,2048]{2,1,0:T(8,128)(2,1)}, u32[]{:S(2)}, u32[]{:S(2)}) async-start(bf16[4,256,2048]{2,1,0:T(8,128)(2,1)} %get-tuple-element.65), calls=%async_computation.1 | async-start | bytes 8388608 | tf_op jit(solution)/shard_map/all_to_all | solution.py:82
  112.9 125.9 %reduce-scatter.3.cloned.1.call-start = ((), (), s32[]{:S(2)}) async-start(), calls=%async_computation.5 | async-start | bytes 4718592 | tf_op jit(solution)/shard_map/reduce_scatter | solution.py:91
  188.4 61.3 %copy-start.4 = (bf16[256,256]{1,0:T(8,128)(2,1)S(1)}, bf16[256,256]{1,0:T(8,128)(2,1)}, u32[]{:S(2)}) copy-start(bf16[256,256]{1,0:T(8,128)(2,1)} %param.27) | copy-start | bytes 393220
  188.4 61.4 %copy-start.5 = (bf16[256,256]{1,0:T(8,128)(2,1)S(1)}, bf16[256,256]{1,0:T(8,128)(2,1)}, u32[]{:S(2)}) copy-start(bf16[256,256]{1,0:T(8,128)(2,1)} %param.26) | copy-start | bytes 393220
  188.4 61.5 %copy-start.6 = (bf16[256,256]{1,0:T(8,128)(2,1)S(1)}, bf16[256,256]{1,0:T(8,128)(2,1)}, u32[]{:S(2)}) copy-start(bf16[256,256]{1,0:T(8,128)(2,1)} %param.25) | copy-start | bytes 393220
  188.4 61.6 %copy-start.7 = (f32[31,256]{1,0:T(8,128)S(1)}, f32[31,256]{1,0:T(8,128)}, u32[]{:S(2)}) copy-start(f32[31,256]{1,0:T(8,128)} %param.24) | copy-start | bytes 95236
  188.4 62.9 %copy-start.47 = (bf16[1024,768]{1,0:T(8,128)(2,1)S(1)}, bf16[1024,768]{1,0:T(8,128)(2,1)}, u32[]{:S(2)}) copy-start(bf16[1024,768]{1,0:T(8,128)(2,1)} %copy-done.46) | copy-start | bytes 4718596
  188.5 107.4 %all-gather.3.cloned.1.call-start = ((), (), s32[]{:S(2)}) async-start(), calls=%async_computation.7 | async-start | bytes 4718592 | tf_op jit(solution)/shard_map/all_gather | solution.py:97
  249.6 112.1 %reduce-scatter.5.cloned.1.call-start = ((), (), s32[]{:S(2)}) async-start(), calls=%async_computation.6 | async-start | bytes 1310720 | tf_op jit(solution)/shard_map/reduce_scatter | solution.py:107
  344.9 11.9 %copy-start.11 = (f32[1,256]{1,0:T(1,128)S(1)}, f32[1,256]{1,0:T(1,128)}, u32[]{:S(2)}) copy-start(f32[1,256]{1,0:T(1,128)} %get-tuple-element.52) | copy-start | bytes 3076
  344.9 11.9 %copy-start.12 = (f32[1,256]{1,0:T(1,128)S(1)}, f32[1,256]{1,0:T(1,128)}, u32[]{:S(2)}) copy-start(f32[1,256]{1,0:T(1,128)} %get-tuple-element.53) | copy-start | bytes 3076
  344.9 11.9 %copy-start.13 = (f32[1,256]{1,0:T(1,128)S(1)}, f32[1,256]{1,0:T(1,128)}, u32[]{:S(2)}) copy-start(f32[1,256]{1,0:T(1,128)} %get-tuple-element.54) | copy-start | bytes 3076
  345.0 11.9 %copy-start.14 = (f32[1,256]{1,0:T(1,128)S(1)}, f32[1,256]{1,0:T(1,128)}, u32[]{:S(2)}) copy-start(f32[1,256]{1,0:T(1,128)} %get-tuple-element.55) | copy-start | bytes 3076
  345.0 11.9 %copy-start.15 = (f32[1,256]{1,0:T(1,128)S(1)}, f32[1,256]{1,0:T(1,128)}, u32[]{:S(2)}) copy-start(f32[1,256]{1,0:T(1,128)} %get-tuple-element.56) | copy-start | bytes 3076
  345.0 11.9 %copy-start.16 = (f32[1,256]{1,0:T(1,128)S(1)}, f32[1,256]{1,0:T(1,128)}, u32[]{:S(2)}) copy-start(f32[1,256]{1,0:T(1,128)} %get-tuple-element.57) | copy-start | bytes 3076
  345.0 11.9 %copy-start.17 = (f32[1,256]{1,0:T(1,128)S(1)}, f32[1,256]{1,0:T(1,128)}, u32[]{:S(2)}) copy-start(f32[1,256]{1,0:T(1,128)} %get-tuple-element.58) | copy-start | bytes 3076
  345.0 11.9 %copy-start.18 = (f32[1,256]{1,0:T(1,128)S(1)}, f32[1,256]{1,0:T(1,128)}, u32[]{:S(2)}) copy-start(f32[1,256]{1,0:T(1,128)} %get-tuple-element.59) | copy-start | bytes 3076
  345.0 11.9 %copy-start.19 = (f32[1,256]{1,0:T(1,128)S(1)}, f32[1,256]{1,0:T(1,128)}, u32[]{:S(2)}) copy-start(f32[1,256]{1,0:T(1,128)} %get-tuple-element.60) | copy-start | bytes 3076
  345.0 11.9 %copy-start.20 = (f32[1,256]{1,0:T(1,128)S(1)}, f32[1,256]{1,0:T(1,128)}, u32[]{:S(2)}) copy-start(f32[1,256]{1,0:T(1,128)} %get-tuple-element.61) | copy-start | bytes 3076
  345.0 11.9 %copy-start.21 = (f32[1,256]{1,0:T(1,128)S(1)}, f32[1,256]{1,0:T(1,128)}, u32[]{:S(2)}) copy-start(f32[1,256]{1,0:T(1,128)} %get-tuple-element.62) | copy-start | bytes 3076
  345.0 11.9 %copy-start.22 = (f32[1,256]{1,0:T(1,128)S(1)}, f32[1,256]{1,0:T(1,128)}, u32[]{:S(2)}) copy-start(f32[1,256]{1,0:T(1,128)} %get-tuple-element.32) | copy-start | bytes 3076
  345.0 11.9 %copy-start.23 = (f32[1,256]{1,0:T(1,128)S(1)}, f32[1,256]{1,0:T(1,128)}, u32[]{:S(2)}) copy-start(f32[1,256]{1,0:T(1,128)} %get-tuple-element.33) | copy-start | bytes 3076
  345.1 11.9 %copy-start.24 = (f32[1,256]{1,0:T(1,128)S(1)}, f32[1,256]{1,0:T(1,128)}, u32[]{:S(2)}) copy-start(f32[1,256]{1,0:T(1,128)} %get-tuple-element.34) | copy-start | bytes 3076
  345.1 11.9 %copy-start.25 = (f32[1,256]{1,0:T(1,128)S(1)}, f32[1,256]{1,0:T(1,128)}, u32[]{:S(2)}) copy-start(f32[1,256]{1,0:T(1,128)} %get-tuple-element.35) | copy-start | bytes 3076
  345.1 11.9 %copy-start.26 = (f32[1,256]{1,0:T(1,128)S(1)}, f32[1,256]{1,0:T(1,128)}, u32[]{:S(2)}) copy-start(f32[1,256]{1,0:T(1,128)} %get-tuple-element.36) | copy-start | bytes 3076
  345.1 11.9 %copy-start.27 = (f32[1,256]{1,0:T(1,128)S(1)}, f32[1,256]{1,0:T(1,128)}, u32[]{:S(2)}) copy-start(f32[1,256]{1,0:T(1,128)} %get-tuple-element.37) | copy-start | bytes 3076
  345.1 11.9 %copy-start.28 = (f32[1,256]{1,0:T(1,128)S(1)}, f32[1,256]{1,0:T(1,128)}, u32[]{:S(2)}) copy-start(f32[1,256]{1,0:T(1,128)} %get-tuple-element.38) | copy-start | bytes 3076
  345.1 11.9 %copy-start.29 = (f32[1,256]{1,0:T(1,128)S(1)}, f32[1,256]{1,0:T(1,128)}, u32[]{:S(2)}) copy-start(f32[1,256]{1,0:T(1,128)} %get-tuple-element.39) | copy-start | bytes 3076
  345.1 11.9 %copy-start.30 = (f32[1,256]{1,0:T(1,128)S(1)}, f32[1,256]{1,0:T(1,128)}, u32[]{:S(2)}) copy-start(f32[1,256]{1,0:T(1,128)} %get-tuple-element.40) | copy-start | bytes 3076
  345.2 11.6 %collective-permute-start = (f32[256,30]{0,1:T(8,128)S(1)}, f32[256,30]{0,1:T(8,128)S(1)}, u32[]{:S(2)}, u32[]{:S(2)}) collective-permute-start(f32[256,30]{0,1:T(8,128)S(1)} %slice.263), channel_id=1, source_target_pairs={{8,0},{16,8},{24,16},{9,1},{17,9},{25,17},{10,2},{18,10},{26,18},{... | collective-permute-start | bytes 92168 | tf_op jit(solution)/shard_map/ppermute | solution.py:13
  348.8 14.8 %copy-start.1 = (bf16[1,2048,768]{2,1,0:T(8,128)(2,1)S(1)}, bf16[1,2048,768]{2,1,0:T(8,128)(2,1)}, u32[]{:S(2)}) copy-start(bf16[1,2048,768]{2,1,0:T(8,128)(2,1)} %param.19) | copy-start | bytes 9437188
  (21 other events, 188.6 us)
Sparse Core Ops, SparseCore 0:
  188.6 50.2 reduce-scatter.2
  249.7 46.1 all-gather.2
  326.2 27.0 reduce-scatter.4
where the time goes:
time: 377 us; the launch traced here: 370 us
  waiting for transfers between devices  113 us (30%)
  blocking collectives  76.3 us (20%)
  matrix products  69.8 us (19%)
  local copies, waits for them, and re-layouts  55.4 us (15%)
  other arithmetic  31.3 us (8%)
  between operations  14.8 us (4%)
  starting transfers between devices  9.92 us (3%)
    dot_general x8, matrix products, contract(): lax.dot_general(left, right, (((left_dim,), (right_dim,)), ((), ())), pre...  57.3 us
    all_to_all x1, blocking collectives, on_device(): lax.all_to_all(send_in, 'sp', split_axis=0, concat_axis=1, tiled=True)  50.8 us
    reduce_scatter x1, waiting for transfers between devices, on_device(): lax.psum_scatter(blocks.astype(jnp.bfloat16), 'tp', scatter_dimension=2,...  50.3 us
    all_to_all x1, waiting for transfers between devices, on_device(): lax.all_to_all(send_cot, 'sp', split_axis=0, concat_axis=1, tiled=True)  32.8 us
    all_gather x1, waiting for transfers between devices, on_device(): lax.all_gather(returned.astype(jnp.bfloat16), 'tp', axis=2, tiled=True)  29.7 us
    psum x1, blocking collectives, on_device(): lax.psum((jnp.sum(norm_cot, axis=0), jnp.sum(norm_cot * centered, axis=0)...  14.7 us
    mul x3, local copies, waits for them, and re-layouts, on_device(): route_weight[:, :, None] * cotangent.astype(jnp.float32)[:, None, :]  11.6 us
    all_to_all x1, blocking collectives, on_device(): lax.all_to_all(share.astype(jnp.bfloat16), 'sp', split_axis=1, concat_axi...  10.8 us
  transfers between devices with their start and end apart: 5, of which 3 were waited for; matrix products, arithmetic and copies ran while one was open for 12% of the time, Pallas kernels for 0%

commit v1 on v0

--- a/solution.py
+++ b/solution.py
@@ -94,7 +94,7 @@
     returned = lax.all_to_all(
         share.astype(jnp.bfloat16), "sp", split_axis=1, concat_axis=0, tiled=True
     ).astype(share.dtype)
-    whole = lax.all_gather(returned.astype(jnp.bfloat16), "tp", axis=2, tiled=True).astype(
+    whole = jnp.concatenate(lax.all_gather(returned.astype(jnp.bfloat16), "tp"), axis=2).astype(
         returned.dtype
     )
     routed = whole.reshape(expert_count * capacity, D)[target].reshape(tokens_here, 2, D)

time: 377 us -> 363 us (0.963)
  matrix products: 69.8 us -> 57.9 us
  other arithmetic: 31.3 us -> 26.3 us
    dot_general x8, matrix products: 57.3 us -> 45.4 us  [contract(): lax.dot_general(left, right, (((left_dim,), (right_dim,)), ((), ())), pre...]
    reshape x1 -> x0, other arithmetic: 6.54 us -> none  [on_device(): whole.reshape(expert_count * capacity, D)[target].reshape(tokens_here, 2, D)]
    convert_element_type x0 -> x1, local copies, waits for them, and re-layouts: none -> 3.86 us  [on_device(): jnp.concatenate(lax.all_gather(returned.astype(jnp.bfloat16), 'tp'), axis=2)]
where the time goes in v1:
time: 363 us; the launch traced here: 357 us
  waiting for transfers between devices  113 us (31%)
  blocking collectives  76.3 us (21%)
  local copies, waits for them, and re-layouts  58.8 us (16%)
  matrix products  57.9 us (16%)
  other arithmetic  26.3 us (7%)
  between operations  14.9 us (4%)
  starting transfers between devices  9.82 us (3%)
    all_to_all x1, blocking collectives, on_device(): lax.all_to_all(send_in, 'sp', split_axis=0, concat_axis=1, tiled=True)  50.8 us
    reduce_scatter x1, waiting for transfers between devices, on_device(): lax.psum_scatter(blocks.astype(jnp.bfloat16), 'tp', scatter_dimension=2,...  50.3 us
    dot_general x8, matrix products, contract(): lax.dot_general(left, right, (((left_dim,), (right_dim,)), ((), ())), pre...  45.4 us
    all_to_all x1, waiting for transfers between devices, on_device(): lax.all_to_all(send_cot, 'sp', split_axis=0, concat_axis=1, tiled=True)  32.7 us
    all_gather x1, waiting for transfers between devices, on_device(): lax.all_gather(returned.astype(jnp.bfloat16), 'tp')  29.7 us
    psum x1, blocking collectives, on_device(): lax.psum((jnp.sum(norm_cot, axis=0), jnp.sum(norm_cot * centered, axis=0)...  14.7 us
    mul x3, local copies, waits for them, and re-layouts, on_device(): route_weight[:, :, None] * cotangent.astype(jnp.float32)[:, None, :]  11.6 us
    all_to_all x1, blocking collectives, on_device(): lax.all_to_all(share.astype(jnp.bfloat16), 'sp', split_axis=1, concat_axi...  10.8 us
  transfers between devices with their start and end apart: 5, of which 3 were waited for; matrix products, arithmetic and copies ran while one was open for 12% of the time, Pallas kernels for 0%

profile of v1, /device:TPU:4, one launch (start us, length us, event | category | flops | bytes accessed | tf_op | source)
XLA Modules:
  0.0 356.7 jit_solution(5410079144028633634)
XLA Ops:
  11.3 2.4 scatter_custom_fusion
  13.8 5.3 %mul.440 = f32[256,2,2048]{2,1,0:T(2,128)} broadcast(bf16[256,2048]{1,0:T(8,128)(2,1)} %param.16), dimensions={0,2} | broadcast | bytes 5242880 | tf_op jit(solution)/shard_map/mul | solution.py:72
  19.1 6.2 %mul.441 = f32[512,2048]{1,0:T(8,128)} reshape(f32[256,2,2048]{2,1,0:T(2,128)} %mul.440) | data formatting | bytes 8388608 | tf_op jit(solution)/shard_map/mul | solution.py:72
  25.6 3.8 %multiply_convert_fusion = bf16[512,2048]{1,0:T(8,128)(2,1)} fusion(f32[512,2048]{1,0:T(8,128)} %mul.441, f32[512]{0:T(512)S(1)} %mul.438), kind=kLoop, calls=%fused_computation.6 | loop fusion | flops 2097152 | bytes 6293504 | tf_op jit(solution)/shard_map/convert_element_type | solution.py:72
  29.4 10.7 %gather_fusion.1 = bf16[1024,2048]{1,0:T(8,128)(2,1)} fusion(bf16[512,2048]{1,0:T(8,128)(2,1)} %multiply_convert_fusion, s32[1024]{0:T(1024)S(1)} %get-tuple-element.63), kind=kCustom, calls=%fused_computation.1 | custom fusion | bytes 8392704 | tf_op jit(solution)/shard_map/gather | solution.py:76
  40.1 10.2 %gather_fusion = bf16[1024,2048]{1,0:T(8,128)(2,1)} fusion(bf16[256,2048]{1,0:T(8,128)(2,1)} %param.15, s32[1024]{0:T(1024)S(1)} %get-tuple-element.64), kind=kCustom, calls=%fused_computation | custom fusion | bytes 8392704 | tf_op jit(solution)/shard_map/gather | solution.py:79
  50.3 5.2 %broadcast_select_fusion = (bf16[4,256,2048]{2,1,0:T(8,128)(2,1)}, bf16[4,256,2048]{2,1,0:T(8,128)(2,1)S(1)}) fusion(bf16[4,256,2048]{2,1,0:T(8,128)(2,1)} %bitcast.107, pred[4,256]{1,0:T(4,128)(4,1)S(1)} %broadcast_in_dim.43, bf16[4,256,2048]{2,1,0:T(8,128)(2,1)} %bitcast.108), kind=kLoop, calls=%fused_computation.7 | loop fusion | flops 4194304 | bytes 16778240 | tf_op jit(solution)/shard_map/jit(_where)/select_n | solution.py:76
  55.4 50.8 %all_to_all.30 = bf16[4,256,2048]{2,1,0:T(8,128)(2,1)} all-to-all(bf16[4,256,2048]{2,1,0:T(8,128)(2,1)S(1)} %get-tuple-element.66), channel_id=1, replica_groups=mesh['sp'=4,'tp'=8] {'sp'}, dimensions={0} | all-to-all | bytes 8388608 | tf_op jit(solution)/shard_map/all_to_all | solution.py:83
  106.3 5.9 %all-to-all-start.1 = ((bf16[4,256,2048]{2,1,0:T(8,128)(2,1)}), bf16[4,256,2048]{2,1,0:T(8,128)(2,1)}, u32[]{:S(2)}, u32[]{:S(2)}) async-start(bf16[4,256,2048]{2,1,0:T(8,128)(2,1)} %get-tuple-element.65), calls=%async_computation.1 | async-start | bytes 8388608 | tf_op jit(solution)/shard_map/all_to_all | solution.py:82
  112.7 7.4 %fusion.2 = f32[1024,768]{1,0:T(8,128)} fusion(bf16[1024,2048]{1,0:T(8,128)(2,1)} %bitcast.109, bf16[1,2048,768]{2,1,0:T(8,128)(2,1)S(1)} %copy-done), kind=kOutput, calls=%fused_computation.43 | convolution fusion | flops 3221225472 | bytes 10485760 | tf_op jit(solution)/shard_map/dot_general | solution.py:23
  120.1 5.1 %fusion.5 = f32[1024,768]{1,0:T(8,128)} fusion(bf16[1024,2048]{1,0:T(8,128)(2,1)S(1)} %bitcast.112, bf16[1,2048,768]{2,1,0:T(8,128)(2,1)S(1)} %copy-done.42), kind=kOutput, calls=%fused_computation.46 | convolution fusion | flops 3221225472 | bytes 10485760 | tf_op jit(solution)/shard_map/dot_general | solution.py:24
  125.2 32.7 %all-to-all-done.1 = bf16[4,256,2048]{2,1,0:T(8,128)(2,1)} async-done(((bf16[4,256,2048]{2,1,0:T(8,128)(2,1)}), bf16[4,256,2048]{2,1,0:T(8,128)(2,1)}, u32[]{:S(2)}, u32[]{:S(2)}) %all-to-all-start.1) | async-done | bytes 4194336 | tf_op jit(solution)/shard_map/all_to_all | solution.py:82
  157.9 9.2 %multiply_convert_fusion.2 = (bf16[1024,768]{1,0:T(8,128)(2,1)S(1)}, bf16[1024,768]{1,0:T(8,128)(2,1)S(1)}) fusion(f32[1024,768]{1,0:T(8,128)} %fusion.2, f32[1024,768]{1,0:T(8,128)} %fusion.5, bf16[1024,2048]{1,0:T(8,128)(2,1)} %bitcast.6, bf16[1,768,2048]{2,1,0:T(8,128)(2,1)} %param.21), kind=kOutput, calls=%fused_computation.51 | convolution fusion | flops 3231449088 | bytes 16777216 | tf_op jit(solution)/shard_map/dot_general | solution.py:17
  167.1 3.4 fusion
  170.6 5.2 %add_convert_fusion = bf16[1024,2048]{1,0:T(8,128)(2,1)} fusion(f32[1024,2048]{1,0:T(8,128)S(1)} %fusion, bf16[1024,768]{1,0:T(8,128)(2,1)S(1)} %get-tuple-element.30, bf16[1,2048,768]{2,1,0:T(8,128)(2,1)S(1)} %copy-done.43), kind=kOutput, calls=%fused_computation.5 | convolution fusion | flops 3225419776 | bytes 17301504 | tf_op jit(solution)/shard_map/dot_general | solution.py:17
  175.9 50.3 %reduce-scatter.3.cloned.1.call-done = bf16[1,4,32,2048]{3,2,0,1:T(8,128)(2,1)} async-done(((bf16[1,4,256,2048]{3,2,0,1:T(8,128)(2,1)}), bf16[1,4,32,2048]{3,2,0,1:T(8,128)(2,1)}) %reduce-scatter.3.cloned.1.call-update) | async-done | bytes 524304 | tf_op jit(solution)/shard_map/reduce_scatter | solution.py:91
  226.2 10.8 %all_to_all.31 = bf16[1,4,32,2048]{3,2,0,1:T(8,128)(2,1)} all-to-all(bf16[1,4,32,2048]{3,2,0,1:T(8,128)(2,1)} %reduce-scatter.3.cloned.1.call-done), channel_id=1, replica_groups=mesh['sp'=4,'tp'=8] {'sp'}, dimensions={1} | all-to-all | bytes 1048576 | tf_op jit(solution)/shard_map/all_to_all | solution.py:94
  238.8 7.5 %fusion.9 = bf16[1,2048,768]{2,1,0:T(8,128)(2,1)} fusion(bf16[1024,2048]{1,0:T(8,128)(2,1)} %bitcast.110, bf16[1024,768]{1,0:T(8,128)(2,1)S(1)} %copy-done.47), kind=kOutput, calls=%fused_computation.54 | convolution fusion | flops 3222798336 | bytes 8912896 | tf_op jit(solution)/shard_map/dot_general | solution.py:17
  246.3 7.3 %fusion.11 = bf16[1,768,2048]{2,1,0:T(8,128)(2,1)} fusion(bf16[1024,2048]{1,0:T(8,128)(2,1)} %bitcast.6, f32[1024,768]{1,0:T(8,128)S(1)} %copy-done.45, f32[1024,768]{1,0:T(8,128)S(1)} %copy-done.44), kind=kOutput, calls=%fused_computation.56 | convolution fusion | flops 3227516928 | bytes 13631488 | tf_op jit(solution)/shard_map/dot_general | solution.py:17
  253.6 29.7 %all-gather.3.cloned.1.call-done = bf16[8,4,32,2048]{3,2,1,0:T(8,128)(2,1)} async-done(((bf16[1,4,32,2048]{3,2,1,0:T(8,128)(2,1)}), bf16[8,4,32,2048]{3,2,1,0:T(8,128)(2,1)}) %all-gather.3.cloned.1.call-update) | async-done | bytes 4194320 | tf_op jit(solution)/shard_map/all_gather | solution.py:97
  283.3 3.2 convert_bitcast_fusion
  286.5 3.9 %copy.43 = f32[4,1,8,32,2048]{4,3,2,0,1:T(8,128)} copy(f32[4,1,8,32,2048]{4,3,0,2,1:T(8,128)S(1)} %convert_bitcast_fusion) | data formatting | bytes 16777216 | tf_op jit(solution)/shard_map/convert_element_type | solution.py:97
  290.4 8.8 %gather_fusion.2 = f32[512,2048]{1,0:T(8,128)} fusion(f32[1024,2048]{1,0:T(8,128)} %bitcast.106, s32[1024]{0:T(1024)S(1)} %pad_clamp_fusion), kind=kCustom, calls=%fused_computation.2 | custom fusion | bytes 8390656 | tf_op jit(solution)/shard_map/gather | solution.py:100
  299.1 6.0 %reshape.158 = f32[256,2,2048]{2,1,0:T(2,128)} reshape(f32[512,2048]{1,0:T(8,128)} %gather_fusion.2) | data formatting | bytes 8388608 | tf_op jit(solution)/shard_map/reshape | solution.py:100
  305.2 7.3 %reduce_sum.40 = f32[256,2048]{1,0:T(8,128)S(1)} reduce(f32[256,2,2048]{2,1,0:T(2,128)} %reshape.158, f32[]{:T(128)} %constant.43.clone.1), dimensions={1}, to_apply=%region_5.6 | reduce | flops 524288 | bytes 6291460 | tf_op jit(solution)/shard_map/reduce_sum | solution.py:101
  312.5 1.7 convolution_convert_fusion.3
  314.3 3.0 fusion.121
  317.2 14.7 %all-reduce = (f32[256]{0:T(256)S(1)}, f32[256]{0:T(256)S(1)}) all-reduce(f32[256]{0:T(256)} %get-tuple-element.25, f32[256]{0:T(256)} %get-tuple-element.24), channel_id=1, replica_groups=mesh['sp'=4,'tp'=8] {'tp'}, use_global_device_ids=true, to_apply=%region_10.11 | all-reduce | flops 512 | bytes 4096 | tf_op jit(solution)/shard_map/psum | solution.py:115
  333.4 3.4 collective-permute-start
  336.8 8.0 %fusion.10 = bf16[1,2048,768]{2,1,0:T(8,128)(2,1)} fusion(bf16[1024,2048]{1,0:T(8,128)(2,1)} %bitcast.111, bf16[1024,768]{1,0:T(8,128)(2,1)} %copy-done.48), kind=kOutput, calls=%fused_computation.55 | convolution fusion | flops 3222798336 | bytes 8912896 | tf_op jit(solution)/shard_map/dot_general | solution.py:17
  345.1 1.5 multiply_convert_fusion.5
  348.2 1.8 convert_element_type.109
  (137 shorter events, 9.6 us)
Async XLA Ops:
  7.2 105.5 %copy-start = (bf16[1,2048,768]{2,1,0:T(8,128)(2,1)S(1)}, bf16[1,2048,768]{2,1,0:T(8,128)(2,1)}, u32[]{:S(2)}) copy-start(bf16[1,2048,768]{2,1,0:T(8,128)(2,1)} %param.19) | copy-start | bytes 9437188
  106.3 51.6 %all-to-all-start.1 = ((bf16[4,256,2048]{2,1,0:T(8,128)(2,1)}), bf16[4,256,2048]{2,1,0:T(8,128)(2,1)}, u32[]{:S(2)}, u32[]{:S(2)}) async-start(bf16[4,256,2048]{2,1,0:T(8,128)(2,1)} %get-tuple-element.65), calls=%async_computation.1 | async-start | bytes 8388608 | tf_op jit(solution)/shard_map/all_to_all | solution.py:82
  112.2 114.0 %reduce-scatter.3.cloned.1.call-start = ((), (), s32[]{:S(2)}) async-start(), calls=%async_computation.5 | async-start | bytes 4718592 | tf_op jit(solution)/shard_map/reduce_scatter | solution.py:91
  175.8 61.3 %copy-start.4 = (bf16[256,256]{1,0:T(8,128)(2,1)S(1)}, bf16[256,256]{1,0:T(8,128)(2,1)}, u32[]{:S(2)}) copy-start(bf16[256,256]{1,0:T(8,128)(2,1)} %param.27) | copy-start | bytes 393220
  175.8 61.4 %copy-start.5 = (bf16[256,256]{1,0:T(8,128)(2,1)S(1)}, bf16[256,256]{1,0:T(8,128)(2,1)}, u32[]{:S(2)}) copy-start(bf16[256,256]{1,0:T(8,128)(2,1)} %param.25) | copy-start | bytes 393220
  175.8 61.5 %copy-start.6 = (bf16[256,256]{1,0:T(8,128)(2,1)S(1)}, bf16[256,256]{1,0:T(8,128)(2,1)}, u32[]{:S(2)}) copy-start(bf16[256,256]{1,0:T(8,128)(2,1)} %param.26) | copy-start | bytes 393220
  175.8 61.6 %copy-start.7 = (f32[31,256]{1,0:T(8,128)S(1)}, f32[31,256]{1,0:T(8,128)}, u32[]{:S(2)}) copy-start(f32[31,256]{1,0:T(8,128)} %param.24) | copy-start | bytes 95236
  175.8 62.9 %copy-start.47 = (bf16[1024,768]{1,0:T(8,128)(2,1)S(1)}, bf16[1024,768]{1,0:T(8,128)(2,1)}, u32[]{:S(2)}) copy-start(bf16[1024,768]{1,0:T(8,128)(2,1)} %copy-done.46) | copy-start | bytes 4718596
  175.8 107.4 %all-gather.3.cloned.1.call-start = ((), (), s32[]{:S(2)}) async-start(), calls=%async_computation.7 | async-start | bytes 4718592 | tf_op jit(solution)/shard_map/all_gather | solution.py:97
  237.0 111.1 %reduce-scatter.5.cloned.1.call-start = ((), (), s32[]{:S(2)}) async-start(), calls=%async_computation.6 | async-start | bytes 1310720 | tf_op jit(solution)/shard_map/reduce_scatter | solution.py:107
  333.1 11.7 %copy-start.11 = (f32[1,256]{1,0:T(1,128)S(1)}, f32[1,256]{1,0:T(1,128)}, u32[]{:S(2)}) copy-start(f32[1,256]{1,0:T(1,128)} %get-tuple-element.52) | copy-start | bytes 3076
  333.1 11.7 %copy-start.12 = (f32[1,256]{1,0:T(1,128)S(1)}, f32[1,256]{1,0:T(1,128)}, u32[]{:S(2)}) copy-start(f32[1,256]{1,0:T(1,128)} %get-tuple-element.53) | copy-start | bytes 3076
  333.1 11.7 %copy-start.13 = (f32[1,256]{1,0:T(1,128)S(1)}, f32[1,256]{1,0:T(1,128)}, u32[]{:S(2)}) copy-start(f32[1,256]{1,0:T(1,128)} %get-tuple-element.54) | copy-start | bytes 3076
  333.1 11.7 %copy-start.14 = (f32[1,256]{1,0:T(1,128)S(1)}, f32[1,256]{1,0:T(1,128)}, u32[]{:S(2)}) copy-start(f32[1,256]{1,0:T(1,128)} %get-tuple-element.55) | copy-start | bytes 3076
  333.1 11.7 %copy-start.15 = (f32[1,256]{1,0:T(1,128)S(1)}, f32[1,256]{1,0:T(1,128)}, u32[]{:S(2)}) copy-start(f32[1,256]{1,0:T(1,128)} %get-tuple-element.56) | copy-start | bytes 3076
  333.1 11.7 %copy-start.16 = (f32[1,256]{1,0:T(1,128)S(1)}, f32[1,256]{1,0:T(1,128)}, u32[]{:S(2)}) copy-start(f32[1,256]{1,0:T(1,128)} %get-tuple-element.57) | copy-start | bytes 3076
  333.2 11.7 %copy-start.17 = (f32[1,256]{1,0:T(1,128)S(1)}, f32[1,256]{1,0:T(1,128)}, u32[]{:S(2)}) copy-start(f32[1,256]{1,0:T(1,128)} %get-tuple-element.58) | copy-start | bytes 3076
  333.2 11.7 %copy-start.18 = (f32[1,256]{1,0:T(1,128)S(1)}, f32[1,256]{1,0:T(1,128)}, u32[]{:S(2)}) copy-start(f32[1,256]{1,0:T(1,128)} %get-tuple-element.59) | copy-start | bytes 3076
  333.2 11.7 %copy-start.19 = (f32[1,256]{1,0:T(1,128)S(1)}, f32[1,256]{1,0:T(1,128)}, u32[]{:S(2)}) copy-start(f32[1,256]{1,0:T(1,128)} %get-tuple-element.60) | copy-start | bytes 3076
  333.2 11.7 %copy-start.20 = (f32[1,256]{1,0:T(1,128)S(1)}, f32[1,256]{1,0:T(1,128)}, u32[]{:S(2)}) copy-start(f32[1,256]{1,0:T(1,128)} %get-tuple-element.61) | copy-start | bytes 3076
  333.2 11.7 %copy-start.21 = (f32[1,256]{1,0:T(1,128)S(1)}, f32[1,256]{1,0:T(1,128)}, u32[]{:S(2)}) copy-start(f32[1,256]{1,0:T(1,128)} %get-tuple-element.62) | copy-start | bytes 3076
  333.2 11.7 %copy-start.22 = (f32[1,256]{1,0:T(1,128)S(1)}, f32[1,256]{1,0:T(1,128)}, u32[]{:S(2)}) copy-start(f32[1,256]{1,0:T(1,128)} %get-tuple-element.32) | copy-start | bytes 3076
  333.2 11.7 %copy-start.23 = (f32[1,256]{1,0:T(1,128)S(1)}, f32[1,256]{1,0:T(1,128)}, u32[]{:S(2)}) copy-start(f32[1,256]{1,0:T(1,128)} %get-tuple-element.33) | copy-start | bytes 3076
  333.2 11.7 %copy-start.24 = (f32[1,256]{1,0:T(1,128)S(1)}, f32[1,256]{1,0:T(1,128)}, u32[]{:S(2)}) copy-start(f32[1,256]{1,0:T(1,128)} %get-tuple-element.34) | copy-start | bytes 3076
  333.2 11.7 %copy-start.25 = (f32[1,256]{1,0:T(1,128)S(1)}, f32[1,256]{1,0:T(1,128)}, u32[]{:S(2)}) copy-start(f32[1,256]{1,0:T(1,128)} %get-tuple-element.35) | copy-start | bytes 3076
  333.2 11.7 %copy-start.26 = (f32[1,256]{1,0:T(1,128)S(1)}, f32[1,256]{1,0:T(1,128)}, u32[]{:S(2)}) copy-start(f32[1,256]{1,0:T(1,128)} %get-tuple-element.36) | copy-start | bytes 3076
  333.3 11.7 %copy-start.27 = (f32[1,256]{1,0:T(1,128)S(1)}, f32[1,256]{1,0:T(1,128)}, u32[]{:S(2)}) copy-start(f32[1,256]{1,0:T(1,128)} %get-tuple-element.37) | copy-start | bytes 3076
  333.3 11.7 %copy-start.28 = (f32[1,256]{1,0:T(1,128)S(1)}, f32[1,256]{1,0:T(1,128)}, u32[]{:S(2)}) copy-start(f32[1,256]{1,0:T(1,128)} %get-tuple-element.38) | copy-start | bytes 3076
  333.3 11.7 %copy-start.29 = (f32[1,256]{1,0:T(1,128)S(1)}, f32[1,256]{1,0:T(1,128)}, u32[]{:S(2)}) copy-start(f32[1,256]{1,0:T(1,128)} %get-tuple-element.39) | copy-start | bytes 3076
  333.3 11.7 %copy-start.30 = (f32[1,256]{1,0:T(1,128)S(1)}, f32[1,256]{1,0:T(1,128)}, u32[]{:S(2)}) copy-start(f32[1,256]{1,0:T(1,128)} %get-tuple-element.40) | copy-start | bytes 3076
  333.4 11.4 %collective-permute-start = (f32[256,30]{0,1:T(8,128)S(1)}, f32[256,30]{0,1:T(8,128)S(1)}, u32[]{:S(2)}, u32[]{:S(2)}) collective-permute-start(f32[256,30]{0,1:T(8,128)S(1)} %slice.263), channel_id=1, source_target_pairs={{8,0},{16,8},{24,16},{9,1},{17,9},{25,17},{10,2},{18,10},{26,18},{... | collective-permute-start | bytes 92168 | tf_op jit(solution)/shard_map/ppermute | solution.py:13
  336.8 13.2 %copy-start.1 = (bf16[1,2048,768]{2,1,0:T(8,128)(2,1)S(1)}, bf16[1,2048,768]{2,1,0:T(8,128)(2,1)}, u32[]{:S(2)}) copy-start(bf16[1,2048,768]{2,1,0:T(8,128)(2,1)} %param.19) | copy-start | bytes 9437188
  (22 other events, 193.0 us)
Sparse Core Ops, SparseCore 0:
  176.0 50.2 reduce-scatter.2
  237.1 46.0 all-gather.2
  314.4 27.0 reduce-scatter.4
